TPU v7x, 128 devices: a whole 4x4x4 slice. The times are simulated.
128 devices in a mesh: sp: 16 (over z, y), tp: 8 (over x, core).
Axes of the slice: x: 4, y: 4, z: 4, core: 2. Of those that a mesh axis runs over, the one named last changes fastest.
Arguments:
- hidden: bfloat16 [6144, 4096], P('sp', 'tp'), may hold values from -6 to 6
- doc_ids: int32 [6144], P('sp'), may hold values from 0 to 7, never falling along the last dimension, each value on 1 to 1536 neighbouring positions
- norm_gain: float32 [3, 4096], replicated, may hold values from 0.1 to 1.9
- w_value: bfloat16 [3, 4096, 2048], P(None, 'sp', 'tp'), may hold values from -0.09375 to 0.09375
- w_gate: bfloat16 [3, 4096, 2048], P(None, 'sp', 'tp'), may hold values from -0.09375 to 0.09375
- conv_taps: float32 [3, 31, 2048], P(None, None, 'tp'), may hold values from -1 to 1
- conv_bias: float32 [3, 2048], P(None, 'tp'), may hold values from -3 to 3
- chan_gain: float32 [3, 2048], P(None, 'tp'), may hold values from 0.1 to 1.9
- chan_bias: float32 [3, 2048], P(None, 'tp'), may hold values from -3 to 3
- w_out: bfloat16 [3, 2048, 4096], P(None, 'sp', 'tp'), may hold values from -0.125 to 0.125
Outputs:
- result: bfloat16 [6144, 4096], P('sp', 'tp')
Inputs may be any that keep to these rules, and one draw needn't show every extreme that they name: `doc_ids`: document numbers never fall along the sequence; each document has 1 to 1536 positions and one has exactly that many.
All inputs are finite; a program needn't handle non-finite values.
Results may differ from a plain program's by a relative error of at most 0.013.
Values may be sent and summed in bfloat16 or wider, within the bound.
No kernel may reach another device: no remote copies, remote signals or barrier semaphores. Data moves between devices by JAX's collectives and lax.ppermute only.
A program may use at most 128 MiB of HBM per device.

v0:
```python
import functools

import jax
import jax.numpy as jnp
from jax import lax
from jax.experimental import pallas as pl
from jax.experimental.pallas import tpu as pltpu
from jax.sharding import Mesh, PartitionSpec as P


LAYERS = 3
T = 192
HALO = 32
TAPS = 31
F32 = jnp.float32
BF16 = jnp.bfloat16

SMEM = pl.BlockSpec(memory_space=pltpu.SMEM)
VMEM = pl.BlockSpec(memory_space=pltpu.VMEM)
HBM = pl.BlockSpec(memory_space=pltpu.HBM)


def swap(a):
    return lax.ppermute(a, "c", [(0, 1), (1, 0)])


def shift(a, by, axis="x"):
    return lax.ppermute(a, axis, [(i, (i + by) % 4) for i in range(4)])


def near(a, b, axis):
    left_a, right_b = shift(a, 1, axis), shift(b, 3, axis)
    left_b, right_a = shift(b, 1, axis), shift(a, 3, axis)
    return a, b, left_a, left_b, right_a, right_b


def far(halves, axis):
    a, b, left_a, left_b, right_a, right_b = halves
    two = shift(left_a, 1, axis), shift(right_b, 3, axis)
    return a, b, left_a, left_b, *two, right_a, right_b


def ring(a, b, axis="x"):
    return far(near(a, b, axis), axis)


def around(a, axis="x"):
    two, one, three = shift(a, 2, axis), shift(a, 1, axis), shift(a, 3, axis)
    return a, one, two, three


def to_all(a, axis):
    n = lax.axis_size(axis)
    return lax.all_to_all(jnp.broadcast_to(a[None], (n, *a.shape)), axis, 0, 0, tiled=True)


def dot(a, b):
    return jnp.dot(a, b, preferred_element_type=F32)


def in_order(w, c):
    return jnp.concatenate([w[2 * c], w[2 * c + 1], w[2 - 2 * c], w[3 - 2 * c]], axis=0)


def first_glu_kernel(ix, xp, gain, *refs):
    value, gate = refs[:8], refs[8:16]
    mine, other, own, oth, xs = refs[16:]
    x, y, z, c = ix[0], ix[1], ix[2], ix[3]
    square = jnp.zeros((2 * T, 256), F32)
    for n in range(16):
        xf = xp[n].astype(F32)
        square = square + xf * xf
        xs[n] = (xf * gain[n]).astype(BF16)
    scale = lax.rsqrt(jnp.sum(square, axis=1, keepdims=True) / 4096.0 + 1e-6)

    def rows(e, d):
        return xs[((z - e) & 3) * 4 + ((y - d) & 3)]

    acc = [jnp.zeros((2 * T, 256), F32)] * 2
    for n in range(4):
        for k, (pieces, at) in enumerate(((value, lambda m: rows(n, m)), (gate, lambda m: rows(m, n)))):
            r = jnp.concatenate([at(m) for m in range(4)], axis=1)
            w = jnp.concatenate([pieces[2 * n + m // 2][m % 2] for m in range(4)], axis=0)
            acc[k] = acc[k] + dot(r, w)
    glu = (acc[0] * scale * jax.nn.sigmoid(acc[1] * scale)).astype(BF16)
    low, high = glu[:T], glu[T:]
    mine[...] = jnp.where(c == 0, low, high)
    other[...] = jnp.where(c == 0, high, low)
    for out, core in ((own, c), (oth, 1 - c)):
        for q in range(2):
            block = xp.at[x * 4 + core * 2 + q]
            out[:, q * 256 : (q + 1) * 256] = jnp.where(c == 0, block[:T, :], block[T:, :])


def first_glu_call(ix, xp, gain, value, gate):
    return pl.pallas_call(
        first_glu_kernel,
        in_specs=[SMEM] + [VMEM] * 18,
        out_specs=[VMEM] * 4,
        scratch_shapes=[pltpu.VMEM((16, 2 * T, 256), BF16)],
        out_shape=[
            *[jax.ShapeDtypeStruct((T, 256), BF16)] * 2,
            *[jax.ShapeDtypeStruct((T, 512), BF16)] * 2,
        ],
        cost_estimate=pl.CostEstimate(
            flops=2 * T * 4096 * 1024, bytes_accessed=8 * 2**20, transcendentals=0
        ),
        compiler_params=pltpu.CompilerParams(vmem_limit_bytes=16 * 2**20),
        name="glu0",
    )(ix, xp, gain.reshape(16, 1, 256), *value, *gate)


def reach_kernel(ix, behind, docs, lim):
    start = (ix[1] == 0) & (ix[2] == 0)
    before = jnp.where(start, -1.0, behind[...].astype(F32))
    ids = jnp.concatenate([before, docs[...].astype(F32)], axis=1)
    reach = jnp.zeros((1, 768), F32)
    for o in range(1, TAPS):
        reach = reach + jnp.where(pltpu.roll(ids, o, 1) == ids, 1.0, 0.0)
    lane = lax.broadcasted_iota(jnp.int32, (T, 384), 1)
    row = lax.broadcasted_iota(jnp.int32, (T, 384), 0)
    spot = jnp.where(lane == row + ix[3] * T, reach[:, 384:], 0.0)
    lim[...] = jnp.broadcast_to(jnp.sum(spot, axis=1, keepdims=True), (T, 128))


def reach_call(ix, behind, docs):
    return pl.pallas_call(
        reach_kernel,
        in_specs=[SMEM, VMEM, VMEM],
        out_specs=VMEM,
        out_shape=jax.ShapeDtypeStruct((T, 128), F32),
        compiler_params=pltpu.CompilerParams(vmem_limit_bytes=2 * 2**20),
        name="reach",
    )(ix, behind.reshape(1, -1), docs.reshape(1, -1))


def fetch(src, row, rows, at, dst, sem):
    first = pl.multiple_of(row * 4, 4)
    copy = pltpu.make_async_copy(src.at[pl.ds(first, 4), pl.ds(at * rows, rows), :], dst, sem)
    copy.start()
    return copy


ARRIVAL = (0, 1, 3, 2)


def glu_kernel(at, ix, *refs):
    xp, gain, w_own, w_oth, own, oth, edge, buf, sem = refs[:8], *refs[8:]
    x, c = ix[0], ix[3]
    copies = [
        fetch(w, (x - d) & 3, 256, at, buf.at[h, n], sem.at[h, n])
        for n, d in enumerate(ARRIVAL)
        for h, w in enumerate((w_own, w_oth))
    ]
    square = jnp.zeros((T, 1), F32)
    acc = [jnp.zeros((T, 512), F32)] * 2
    for n, d in enumerate(ARRIVAL):
        parts = []
        for h, core in ((0, c), (1, 1 - c)):
            xf = xp[2 * d + h][...].astype(F32)
            square = square + jnp.sum(xf * xf, axis=1, keepdims=True)
            parts.append((xf * gain[((x - d) & 3) * 2 + core]).astype(BF16))
        rows = jnp.concatenate(parts, axis=1)
        for h in range(2):
            copies[2 * n + h].wait()
            acc[h] = acc[h] + dot(rows, in_order(buf.at[h, n], c))
    scale = lax.rsqrt(square / 4096.0 + 1e-6)
    for h, out in enumerate((own, oth)):
        y = acc[h] * scale
        glu = (y[:, :256] * jax.nn.sigmoid(y[:, 256:])).astype(BF16)
        out[...] = glu
        edge[h * HALO : (h + 1) * HALO, :] = glu[T - HALO :, :]


def glu_call(ix, xp, gain, w_own, w_oth, at):
    return pl.pallas_call(
        functools.partial(glu_kernel, at),
        in_specs=[SMEM] + [VMEM] * 9 + [HBM, HBM],
        out_specs=[VMEM] * 3,
        scratch_shapes=[
            pltpu.VMEM((2, 4, 4, 256, 512), BF16),
            pltpu.SemaphoreType.DMA((2, 4)),
        ],
        out_shape=[
            jax.ShapeDtypeStruct((T, 256), BF16),
            jax.ShapeDtypeStruct((T, 256), BF16),
            jax.ShapeDtypeStruct((2 * HALO, 256), BF16),
        ],
        cost_estimate=pl.CostEstimate(
            flops=2 * T * 4096 * 1024, bytes_accessed=10 * 2**20, transcendentals=0
        ),
        compiler_params=pltpu.CompilerParams(vmem_limit_bytes=16 * 2**20),
        name="glu",
    )(ix, *xp, gain.reshape(8, 1, 512), w_own, w_oth)


def thirds(v):
    high = v.astype(BF16)
    rest = v - high.astype(F32)
    middle = rest.astype(BF16)
    return high, middle, (rest - middle.astype(F32)).astype(BF16)


def conv_kernel(l, edge, own, oth, lim, chan_own, chan_oth, out, ext):
    chan = (chan_own, chan_own, chan_oth, chan_oth)
    cols = (slice(0, 128), slice(128, 256)) * 2
    for j in range(4):
        ext[j, HALO:, :] = (own, oth)[j // 2][:, cols[j]].astype(F32)
        rows = slice((1 - j // 2) * HALO, (2 - j // 2) * HALO)
        ext[j, :HALO, :] = edge[rows, cols[j]].astype(F32)
    lane = lax.broadcasted_iota(jnp.int32, (32, 128), 1)
    row = lax.broadcasted_iota(jnp.int32, (32, 128), 0)
    pick = lax.broadcasted_iota(jnp.int32, (16, 128), 0)

    def chunk(n, tail):
        r = pl.multiple_of(n * 32, 32)
        reach = lim[pl.ds(r, 32), :]
        acc = [jnp.broadcast_to(chan[j][l, TAPS : TAPS + 1, cols[j]], (32, 128)) for j in range(4)]
        for i in range(TAPS):
            keep = reach >= float(TAPS - 1 - i)
            for j in range(4):
                term = ext[j, pl.ds(r + (HALO - TAPS + 1 + i), 32), :]
                term = term * chan[j][l, i : i + 1, cols[j]]
                acc[j] = acc[j] + jnp.where(keep, term, 0.0)
        mean = jnp.sum(acc[0] + acc[1] + acc[2] + acc[3], axis=1, keepdims=True) / 512.0
        mean = mean.astype(BF16).astype(F32)
        for j in range(4):
            out[pl.ds(r, 32), j * 128 : (j + 1) * 128] = (acc[j] - mean).astype(BF16)
        spot = jnp.where(lane == row + n % 4 * 32, mean, 0.0)
        spot = jnp.sum(spot, axis=0, keepdims=True)
        return tail + jnp.where(pick == n // 4, spot, 0.0)

    tail = lax.fori_loop(0, T // 32, chunk, jnp.zeros((16, 128), F32)).astype(BF16)
    for j in range(4):
        block = tail if j == 0 else jnp.zeros((16, 128), BF16)
        at = 2
        for k in (1, 2):
            for part in thirds(chan[j][l, TAPS + k : TAPS + k + 1, cols[j]]):
                block = jnp.where(pick == at, jnp.broadcast_to(part.astype(F32), (16, 128)), block.astype(F32)).astype(BF16)
                at += 1
        out[T:, j * 128 : (j + 1) * 128] = block


def conv_call(l, *args):
    return pl.pallas_call(
        functools.partial(conv_kernel, l),
        out_shape=jax.ShapeDtypeStruct((T + 16, 512), BF16),
        scratch_shapes=[pltpu.VMEM((4, HALO + T, 128), F32)],
        cost_estimate=pl.CostEstimate(flops=10**9, bytes_accessed=2**20, transcendentals=0),
        compiler_params=pltpu.CompilerParams(vmem_limit_bytes=6 * 2**20),
        name="conv",
    )(*args)


def mix_kernel(at, ix, *refs):
    cp, state, refs = refs[:4], refs[4:6], refs[6:]
    weights, outs, (mixed, buf, sem) = refs[:2], refs[2:4], refs[4:]
    x, c = ix[0], ix[3]
    copies = [
        fetch(w, (x - d) & 3, 128, at[h], buf.at[h, n], sem.at[h, n])
        for n, d in enumerate(ARRIVAL)
        for h, w in enumerate(weights)
    ]
    lane = lax.broadcasted_iota(jnp.int32, (64, 128), 1)
    row = lax.broadcasted_iota(jnp.int32, (64, 128), 0)

    def chunk(n, carry):
        r = pl.multiple_of(n * 64, 64)
        spot = lane == row + n % 2 * 64
        means, total = [], jnp.zeros((64, 128), F32)

        def part(d, k):
            return cp[d][pl.ds(r, 64), k * 128 : (k + 1) * 128].astype(F32) + means[d]

        for d in range(4):
            tail = cp[d][T : T + 16, :128].astype(F32)
            mine = jnp.where(n < 2, tail[0:1, :], tail[1:2, :])
            means.append(jnp.sum(jnp.where(spot, mine, 0.0), axis=1, keepdims=True))
            for k in range(4):
                total = total + part(d, k)
        mu = jnp.sum(total, axis=1, keepdims=True) / 2048.0
        square = jnp.zeros((64, 128), F32)
        for d in range(4):
            for k in range(4):
                off = part(d, k) - mu
                square = square + off * off
        inv = lax.rsqrt(jnp.sum(square, axis=1, keepdims=True) / 2048.0 + 1e-5)
        for d in range(4):
            for k in range(4):
                at = slice(k * 128, (k + 1) * 128)
                tail = cp[d][T:, at].astype(F32)
                gain, bias = [jnp.sum(tail[m : m + 3, :], axis=0, keepdims=True) for m in (2, 5)]
                v = (part(d, k) - mu) * inv * gain + bias
                mixed[d, pl.ds(r, 64), at] = (v * jax.nn.sigmoid(v)).astype(BF16)
        return carry

    lax.fori_loop(0, T // 64, chunk, 0)
    acc = [jnp.zeros((T, 512), F32)] * 2
    for n, d in enumerate(ARRIVAL):
        for h in range(2):
            copies[2 * n + h].wait()
            acc[h] = acc[h] + dot(mixed[d], in_order(buf.at[h, n], c))
    for h in range(2):
        outs[h][...] = (state[h][...].astype(F32) + acc[h]).astype(BF16)


def mix_call(ix, cp, state, weights, at):
    return pl.pallas_call(
        functools.partial(mix_kernel, at),
        in_specs=[SMEM] + [VMEM] * 6 + [HBM] * 2,
        out_specs=[VMEM] * 2,
        scratch_shapes=[
            pltpu.VMEM((4, T, 512), BF16),
            pltpu.VMEM((2, 4, 4, 128, 512), BF16),
            pltpu.SemaphoreType.DMA((2, 4)),
        ],
        out_shape=[jax.ShapeDtypeStruct((T, 512), BF16)] * 2,
        cost_estimate=pl.CostEstimate(
            flops=2 * T * 2048 * 1024, bytes_accessed=6 * 2**20, transcendentals=0
        ),
        compiler_params=pltpu.CompilerParams(vmem_limit_bytes=12 * 2**20),
        name="mix",
    )(ix, *cp, *state, *weights)


def layers(
    hidden, doc_ids, norm_gain, w_value, w_gate, conv_taps, conv_bias, chan_gain, chan_bias, w_out
):
    x, y, z, c = (lax.axis_index(n) for n in ("x", "y", "z", "c"))
    ix = jnp.stack([x, y, z, c]).astype(jnp.int32)

    def pair(l):
        return jnp.concatenate([w_value[l], w_gate[l]], axis=1)

    def all_rows(*parts):
        return lax.all_gather(jnp.concatenate(parts, axis=0), ("z", "y"), axis=0)

    middle = all_rows(pair(1), w_out[0], w_out[1])
    blocks = jnp.moveaxis(hidden.reshape(2 * T, 2, 256), 1, 0)
    first = to_all(blocks, ("x", "c")).reshape(16, 2 * T, 256)

    value, gate = around(w_value[0], "y"), around(w_gate[0], "z")
    value, gate = jnp.stack(value), jnp.stack(gate)
    value, gate = near(value[:2], value[2:], "z"), near(gate[:2], gate[2:], "y")
    value, gate = far(value, "z"), far(gate, "y")

    onward = [(i, i + 1) for i in range(15)]
    behind = lax.ppermute(doc_ids, ("z", "y"), onward)
    lim = reach_call(ix, behind, doc_ids)
    rows = [v[:, None] for v in (conv_bias, chan_gain, chan_bias)]
    chan = jnp.concatenate([conv_taps, *rows], axis=1)
    chan = (chan, swap(chan))
    parts = jnp.concatenate([pair(2), w_out[2]], axis=0)
    last = all_rows(parts)

    onward = [(i, i + 1) for i in range(31)]
    for l in range(LAYERS):
        if l == 0:
            own, oth, *state = first_glu_call(ix, first, norm_gain[l], value, gate)
            oth = swap(oth)
            edge = jnp.concatenate([own[-HALO:], oth[-HALO:]], axis=0)
        else:
            weights = weights if l == 1 else last
            own, oth, edge = glu_call(ix, ring(*state), norm_gain[l], *weights, 0)
        edge = lax.ppermute(edge, ("z", "y", "c"), onward)
        dev = conv_call(l, edge, own, oth, lim, *chan)
        if l == 0:
            part = middle[:, 256:384]
            part = swap(part)
            middle, part = lax.optimization_barrier((middle, part))
            weights = (middle, swap(middle))
        devs = around(dev)
        with_out = ((middle, part), (2, 0)) if l == 0 else (weights, (4 - l, 4 - l))
        state = mix_call(ix, devs, state, *with_out)
        if l == 1:
            last, *state = lax.optimization_barrier((last, *state))
            last = (last, swap(last))

    own, oth = state[0], swap(state[1])
    low = jnp.where(c == 0, own, oth)
    high = jnp.where(c == 0, oth, own)
    return jnp.concatenate([low, high], axis=0)


def solution(mesh):
    fine = Mesh(mesh.devices.reshape(4, 4, 4, 2), ("z", "y", "x", "c"))
    sp, tp = ("z", "y"), ("x", "c")
    placed = (
        P(sp, tp),
        P(sp),
        P(),
        P(None, sp, tp),
        P(None, sp, tp),
        P(None, None, tp),
        P(None, tp),
        P(None, tp),
        P(None, tp),
        P(None, sp, tp),
    )
    return jax.shard_map(layers, mesh=fine, in_specs=placed, out_specs=P(sp, tp), check_vma=False)
```

profile of v0, /device:TPU:32, one launch (start us, length us, event | category | flops | bytes accessed | tf_op | source)
XLA Modules:
  0.0 308.7 jit_solution(4201170139785221181)
XLA Ops:
  11.4 72.1 %all-gather.7.cloned.1.call-done = bf16[8192,512]{1,0:T(8,128)(2,1)} async-done(((bf16[512,512]{1,0:T(8,128)(2,1)}), bf16[8192,512]{1,0:T(8,128)(2,1)}) %all-gather.7.cloned.1.call-update) | async-done | bytes 8388624 | tf_op jit(solution)/shard_map/all_gather | solution.py:336
  85.3 4.1 %collective-permute-done.25.refs_7_ = bf16[16,128,512]{2,1,0:T(8,128)(2,1)S(1)} collective-permute-done((bf16[16,128,512]{2,1,0:T(8,128)(2,1)S(1)}, bf16[16,128,512]{2,1,0:T(8,128)(2,1)S(1)}, u32[]{:S(2)}, u32[]{:S(2)}) %collective-permute-start.25) | collective-permute-done | bytes 2097184 | tf_op jit(solution)/shard_map/ppermute | solution.py:24
  93.2 4.3 %all-to-all-start = ((bf16[8,2,384,256]{3,2,1,0:T(8,128)(2,1)}), bf16[8,2,384,256]{3,2,1,0:T(8,128)(2,1)S(1)}, u32[]{:S(2)}, u32[]{:S(2)}) async-start(bf16[8,2,384,256]{3,2,1,0:T(8,128)(2,1)} %broadcast_in_dim.15), calls=%async_computation | async-start | bytes 6291456 | tf_op jit(solution)/shard_map/all_to_all | solution.py:54
  104.1 3.9 %collective-permute-done.10 = bf16[256,256]{1,0:T(8,128)(2,1)S(1)} collective-permute-done((bf16[256,256]{1,0:T(8,128)(2,1)}, bf16[256,256]{1,0:T(8,128)(2,1)S(1)}, u32[]{:S(2)}, u32[]{:S(2)}) %collective-permute-start.10) | collective-permute-done | bytes 131104 | tf_op jit(solution)/shard_map/ppermute | solution.py:28
  111.2 3.0 collective-permute-start.15
  126.4 5.2 %collective-permute-done.4.refs_3_ = bf16[2,256,256]{2,1,0:T(8,128)(2,1)S(1)} collective-permute-done((bf16[2,256,256]{2,1,0:T(8,128)(2,1)S(1)}, bf16[2,256,256]{2,1,0:T(8,128)(2,1)S(1)}, u32[]{:S(2)}, u32[]{:S(2)}) %collective-permute-start.4) | collective-permute-done | bytes 262176 | tf_op jit(solution)/shard_map/ppermute | solution.py:28
  137.5 3.8 %collective-permute-done.3.refs_2_ = bf16[2,256,256]{2,1,0:T(8,128)(2,1)} collective-permute-done((bf16[2,256,256]{2,1,0:T(8,128)(2,1)S(1)}, bf16[2,256,256]{2,1,0:T(8,128)(2,1)}, u32[]{:S(2)}, u32[]{:S(2)}) %collective-permute-start.3) | collective-permute-done | bytes 262176 | tf_op jit(solution)/shard_map/ppermute | solution.py:28
  143.1 3.4 %collective-permute-done.8.refs_6_ = bf16[2,256,256]{2,1,0:T(8,128)(2,1)S(1)} collective-permute-done((bf16[2,256,256]{2,1,0:T(8,128)(2,1)S(1)}, bf16[2,256,256]{2,1,0:T(8,128)(2,1)S(1)}, u32[]{:S(2)}, u32[]{:S(2)}) %collective-permute-start.8) | collective-permute-done | bytes 262176 | tf_op jit(solution)/shard_map/ppermute | solution.py:28
  149.4 6.6 %collective-permute-done.7.refs_5_ = bf16[2,256,256]{2,1,0:T(8,128)(2,1)} collective-permute-done((bf16[2,256,256]{2,1,0:T(8,128)(2,1)}, bf16[2,256,256]{2,1,0:T(8,128)(2,1)}, u32[]{:S(2)}, u32[]{:S(2)}) %collective-permute-start.7) | collective-permute-done | bytes 262176 | tf_op jit(solution)/shard_map/ppermute | solution.py:28
  156.4 3.2 %collective-permute-done.5.refs_4_ = bf16[2,256,256]{2,1,0:T(8,128)(2,1)} collective-permute-done((bf16[2,256,256]{2,1,0:T(8,128)(2,1)}, bf16[2,256,256]{2,1,0:T(8,128)(2,1)}, u32[]{:S(2)}, u32[]{:S(2)}) %collective-permute-start.5) | collective-permute-done | bytes 262176 | tf_op jit(solution)/shard_map/ppermute | solution.py:28
  166.5 4.5 %glu0.1 = (bf16[192,256]{1,0:T(8,128)(2,1)S(1)}, bf16[192,256]{1,0:T(8,128)(2,1)S(1)}, bf16[192,512]{1,0:T(8,128)(2,1)S(1)}, bf16[192,512]{1,0:T(8,128)(2,1)S(1)}) custom-call(s32[4]{0:T(128)S(1)} %pad_add_fusion.ix, bf16[16,384,256]{2,1,0:T(8,128)(2,1)S(1)} %bitcast.45, f32[16,1,256]{2,1,0:T(1,128)S(1)} %bitcast.48, bf16[2,256,256]{2,1,0:T(8,128)(2,1)S(1)} %copy-done.10, ...), custom_call_target="tpu_custom_call" | custom-call | flops 1610612736 | bytes 8388608 | tf_op jit(solution)/shard_map/glu0/pallas_call | solution.py:96
  176.4 5.6 %collective-permute-done.20 = s32[384]{0:T(512)S(1)} collective-permute-done((s32[384]{0:T(512)S(1)}, s32[384]{0:T(512)S(1)}, u32[]{:S(2)}, u32[]{:S(2)}) %collective-permute-start.20) | collective-permute-done | bytes 1568 | tf_op jit(solution)/shard_map/ppermute | solution.py:348
  194.1 5.4 %collective-permute-done.23.refs_2_ = bf16[208,512]{1,0:T(8,128)(2,1)S(1)} collective-permute-done((bf16[208,512]{1,0:T(8,128)(2,1)S(1)}, bf16[208,512]{1,0:T(8,128)(2,1)S(1)}, u32[]{:S(2)}, u32[]{:S(2)}) %collective-permute-start.23) | collective-permute-done | bytes 213024 | tf_op jit(solution)/shard_map/ppermute | solution.py:28
  199.5 3.4 %copy-done = bf16[8192,512]{1,0:T(8,128)(2,1)S(1)} copy-done((bf16[8192,512]{1,0:T(8,128)(2,1)S(1)}, bf16[8192,512]{1,0:T(8,128)(2,1)}, u32[]{:S(2)}) %copy-start) | copy-done | bytes 8388632
  202.9 3.8 %mix.3 = (bf16[192,512]{1,0:T(8,128)(2,1)S(1)}, bf16[192,512]{1,0:T(8,128)(2,1)S(1)}) custom-call(s32[4]{0:T(128)S(1)} %pad_add_fusion.ix, bf16[208,512]{1,0:T(8,128)(2,1)S(1)} %conv.3.refs_0_, bf16[208,512]{1,0:T(8,128)(2,1)S(1)} %collective-permute-done.22.refs_1_, bf16[208,512]{1,0:T(8,128)(2,1)S(1)} %collective-permute-done.23.refs_2_, ...), custom_call_target="tpu_custom_call" | custom-call | flops 805306368 | bytes 6291456 | tf_op jit(solution)/shard_map/mix/pallas_call | solution.py:308
  210.0 3.2 %collective-permute-start.31 = (bf16[192,512]{1,0:T(8,128)(2,1)S(1)}, bf16[192,512]{1,0:T(8,128)(2,1)S(1)}, u32[]{:S(2)}, u32[]{:S(2)}) collective-permute-start(bf16[192,512]{1,0:T(8,128)(2,1)S(1)} %get-tuple-element.32.refs_0_.refs_4_), channel_id=1, source_target_pairs={{0,6},{2,0},{4,2},{6,4},{1,7},{3,1},{5,3},{7,5},{8,14},{10,8},{12,... | collective-permute-start | bytes 589832 | tf_op jit(solution)/shard_map/ppermute | solution.py:28
  215.8 2.9 collective-permute-start.30
  222.2 4.4 %glu.2 = (bf16[192,256]{1,0:T(8,128)(2,1)S(1)}, bf16[192,256]{1,0:T(8,128)(2,1)S(1)}, bf16[64,256]{1,0:T(8,128)(2,1)S(1)}) custom-call(s32[4]{0:T(128)S(1)} %pad_add_fusion.ix, bf16[192,512]{1,0:T(8,128)(2,1)S(1)} %get-tuple-element.32.refs_0_.refs_4_, bf16[192,512]{1,0:T(8,128)(2,1)S(1)} %get-tuple-element.33.refs_1_.refs_5_, ...), custom_call_target="tpu_custom_call" | custom-call | flops 1610612736 | bytes 10485760 | tf_op jit(solution)/shard_map/glu/pallas_call | solution.py:176
  228.6 5.4 %collective-permute-done.33.edge = bf16[64,256]{1,0:T(8,128)(2,1)S(1)} collective-permute-done((bf16[64,256]{1,0:T(8,128)(2,1)S(1)}, bf16[64,256]{1,0:T(8,128)(2,1)S(1)}, u32[]{:S(2)}, u32[]{:S(2)}) %collective-permute-start.33) | collective-permute-done | bytes 32800 | tf_op jit(solution)/shard_map/ppermute | solution.py:365
  237.7 3.9 %collective-permute-start.35 = (bf16[208,512]{1,0:T(8,128)(2,1)S(1)}, bf16[208,512]{1,0:T(8,128)(2,1)S(1)}, u32[]{:S(2)}, u32[]{:S(2)}) collective-permute-start(bf16[208,512]{1,0:T(8,128)(2,1)S(1)} %conv.4.refs_0_), channel_id=1, source_target_pairs={{0,4},{2,6},{4,0},{6,2},{1,5},{3,7},{5,1},{7,3},{8,12},{10,14},{12... | collective-permute-start | bytes 638984 | tf_op jit(solution)/shard_map/ppermute | solution.py:28
  244.7 2.9 collective-permute-done.35.refs_2_
  247.7 3.6 %mix.4 = (bf16[192,512]{1,0:T(8,128)(2,1)S(1)}, bf16[192,512]{1,0:T(8,128)(2,1)S(1)}) custom-call(s32[4]{0:T(128)S(1)} %pad_add_fusion.ix, bf16[208,512]{1,0:T(8,128)(2,1)S(1)} %conv.4.refs_0_, bf16[208,512]{1,0:T(8,128)(2,1)S(1)} %collective-permute-done.34.refs_1_, bf16[208,512]{1,0:T(8,128)(2,1)S(1)} %collective-permute-done.35.refs_2_, ...), custom_call_target="tpu_custom_call" | custom-call | flops 805306368 | bytes 6291456 | tf_op jit(solution)/shard_map/mix/pallas_call | solution.py:308
  254.9 3.1 collective-permute-start.42
  260.7 3.1 collective-permute-start.41
  264.9 3.5 %collective-permute-done.39.refs_4_ = bf16[192,512]{1,0:T(8,128)(2,1)S(1)} collective-permute-done((bf16[192,512]{1,0:T(8,128)(2,1)S(1)}, bf16[192,512]{1,0:T(8,128)(2,1)S(1)}, u32[]{:S(2)}, u32[]{:S(2)}) %collective-permute-start.39) | collective-permute-done | bytes 196640 | tf_op jit(solution)/shard_map/ppermute | solution.py:28
  268.4 2.8 copy-done.1
  271.2 3.9 %glu.3 = (bf16[192,256]{1,0:T(8,128)(2,1)S(1)}, bf16[192,256]{1,0:T(8,128)(2,1)S(1)}, bf16[64,256]{1,0:T(8,128)(2,1)S(1)}) custom-call(s32[4]{0:T(128)S(1)} %pad_add_fusion.ix, bf16[192,512]{1,0:T(8,128)(2,1)S(1)} %get-tuple-element.39.refs_0_.refs_4_, bf16[192,512]{1,0:T(8,128)(2,1)S(1)} %get-tuple-element.40.refs_1_.refs_5_, ...), custom_call_target="tpu_custom_call" | custom-call | flops 1610612736 | bytes 10485760 | tf_op jit(solution)/shard_map/glu/pallas_call | solution.py:176
  277.0 5.4 %collective-permute-done.44.edge = bf16[64,256]{1,0:T(8,128)(2,1)S(1)} collective-permute-done((bf16[64,256]{1,0:T(8,128)(2,1)S(1)}, bf16[64,256]{1,0:T(8,128)(2,1)S(1)}, u32[]{:S(2)}, u32[]{:S(2)}) %collective-permute-start.44) | collective-permute-done | bytes 32800 | tf_op jit(solution)/shard_map/ppermute | solution.py:365
  285.7 3.9 %collective-permute-start.46 = (bf16[208,512]{1,0:T(8,128)(2,1)S(1)}, bf16[208,512]{1,0:T(8,128)(2,1)S(1)}, u32[]{:S(2)}, u32[]{:S(2)}) collective-permute-start(bf16[208,512]{1,0:T(8,128)(2,1)S(1)} %conv.5.refs_0_), channel_id=1, source_target_pairs={{0,4},{2,6},{4,0},{6,2},{1,5},{3,7},{5,1},{7,3},{8,12},{10,14},{12... | collective-permute-start | bytes 638984 | tf_op jit(solution)/shard_map/ppermute | solution.py:28
  290.0 2.8 collective-permute-done.45.refs_1_
  292.8 2.9 collective-permute-done.46.refs_2_
  295.7 3.8 %mix.5 = (bf16[192,512]{1,0:T(8,128)(2,1)S(1)}, bf16[192,512]{1,0:T(8,128)(2,1)S(1)}) custom-call(s32[4]{0:T(128)S(1)} %pad_add_fusion.ix, bf16[208,512]{1,0:T(8,128)(2,1)S(1)} %conv.5.refs_0_, bf16[208,512]{1,0:T(8,128)(2,1)S(1)} %collective-permute-done.45.refs_1_, bf16[208,512]{1,0:T(8,128)(2,1)S(1)} %collective-permute-done.46.refs_2_, ...), custom_call_target="tpu_custom_call" | custom-call | flops 805306368 | bytes 6291456 | tf_op jit(solution)/shard_map/mix/pallas_call | solution.py:308
  (166 shorter events, 101.0 us)
Async XLA Ops:
  6.5 76.9 %all-gather.7.cloned.1.call-start = ((), (), s32[]{:S(2)}) async-start(), calls=%async_computation.2 | async-start | bytes 8912896 | tf_op jit(solution)/shard_map/all_gather | solution.py:336
  10.5 240.8 %all-gather.5.cloned.1.call-start = ((), (), s32[]{:S(2)}) async-start(), calls=%async_computation.1 | async-start | bytes 6684672 | tf_op jit(solution)/shard_map/all_gather | solution.py:336
  90.8 131.4 %collective-permute-start.32 = (bf16[16,512,512]{2,1,0:T(8,128)(2,1)}, bf16[16,512,512]{2,1,0:T(8,128)(2,1)}, u32[]{:S(2)}, u32[]{:S(2)}) collective-permute-start(bf16[16,512,512]{2,1,0:T(8,128)(2,1)} %bitcast.36), channel_id=1, source_target_pairs={{0,1},{1,0},{2,3},{3,2},{4,5},{5,4},{6,7},{7,6},{8,9},{9,8},{10,11... | collective-permute-start | bytes 25165832 | tf_op jit(solution)/shard_map/ppermute | solution.py:24
  93.2 66.4 %all-to-all-start = ((bf16[8,2,384,256]{3,2,1,0:T(8,128)(2,1)}), bf16[8,2,384,256]{3,2,1,0:T(8,128)(2,1)S(1)}, u32[]{:S(2)}, u32[]{:S(2)}) async-start(bf16[8,2,384,256]{3,2,1,0:T(8,128)(2,1)} %broadcast_in_dim.15), calls=%async_computation | async-start | bytes 6291456 | tf_op jit(solution)/shard_map/all_to_all | solution.py:54
  97.5 10.5 %collective-permute-start.10 = (bf16[256,256]{1,0:T(8,128)(2,1)}, bf16[256,256]{1,0:T(8,128)(2,1)S(1)}, u32[]{:S(2)}, u32[]{:S(2)}) collective-permute-start(bf16[256,256]{1,0:T(8,128)(2,1)} %get-tuple-element.54), channel_id=1, source_target_pairs={{0,64},{32,96},{64,0},{96,32},{1,65},{33,97},{65,1},{97,33},{2,66}... | collective-permute-start | bytes 393224 | tf_op jit(solution)/shard_map/ppermute | solution.py:28
  99.8 11.0 %collective-permute-start.11 = (bf16[256,256]{1,0:T(8,128)(2,1)}, bf16[256,256]{1,0:T(8,128)(2,1)S(1)}, u32[]{:S(2)}, u32[]{:S(2)}) collective-permute-start(bf16[256,256]{1,0:T(8,128)(2,1)} %get-tuple-element.54), channel_id=1, source_target_pairs={{0,96},{32,0},{64,32},{96,64},{1,97},{33,1},{65,33},{97,65},{2,98}... | collective-permute-start | bytes 393224 | tf_op jit(solution)/shard_map/ppermute | solution.py:28
  101.2 10.0 %collective-permute-start.1 = (bf16[256,256]{1,0:T(8,128)(2,1)}, bf16[256,256]{1,0:T(8,128)(2,1)S(1)}, u32[]{:S(2)}, u32[]{:S(2)}) collective-permute-start(bf16[256,256]{1,0:T(8,128)(2,1)} %get-tuple-element.65), channel_id=1, source_target_pairs={{0,16},{8,24},{16,0},{24,8},{1,17},{9,25},{17,1},{25,9},{2,18},{10... | collective-permute-start | bytes 393224 | tf_op jit(solution)/shard_map/ppermute | solution.py:28
  102.7 11.4 %collective-permute-start.2 = (bf16[256,256]{1,0:T(8,128)(2,1)}, bf16[256,256]{1,0:T(8,128)(2,1)S(1)}, u32[]{:S(2)}, u32[]{:S(2)}) collective-permute-start(bf16[256,256]{1,0:T(8,128)(2,1)} %get-tuple-element.65), channel_id=1, source_target_pairs={{0,24},{8,0},{16,8},{24,16},{1,25},{9,1},{17,9},{25,17},{2,26},{10... | collective-permute-start | bytes 393224 | tf_op jit(solution)/shard_map/ppermute | solution.py:28
  111.2 9.3 %collective-permute-start.15 = (bf16[2,256,256]{2,1,0:T(8,128)(2,1)S(1)}, bf16[2,256,256]{2,1,0:T(8,128)(2,1)}, u32[]{:S(2)}, u32[]{:S(2)}) collective-permute-start(bf16[2,256,256]{2,1,0:T(8,128)(2,1)S(1)} %pad_maximum_fusion.6.refs_9_), channel_id=1, source_target_pairs={{0,24},{8,0},{16,8},{24,16},{1,25},{9,1},{17,9},{25,17},{2,26},{10... | collective-permute-start | bytes 786440 | tf_op jit(solution)/shard_map/ppermute | solution.py:28
  117.7 13.9 %collective-permute-start.4 = (bf16[2,256,256]{2,1,0:T(8,128)(2,1)S(1)}, bf16[2,256,256]{2,1,0:T(8,128)(2,1)S(1)}, u32[]{:S(2)}, u32[]{:S(2)}) collective-permute-start(bf16[2,256,256]{2,1,0:T(8,128)(2,1)S(1)} %pad_maximum_fusion.4.refs_1_), channel_id=1, source_target_pairs={{0,32},{32,64},{64,96},{96,0},{1,33},{33,65},{65,97},{97,1},{2,34}... | collective-permute-start | bytes 786440 | tf_op jit(solution)/shard_map/ppermute | solution.py:28
  120.5 14.6 %collective-permute-start.12 = (bf16[2,256,256]{2,1,0:T(8,128)(2,1)S(1)}, bf16[2,256,256]{2,1,0:T(8,128)(2,1)}, u32[]{:S(2)}, u32[]{:S(2)}) collective-permute-start(bf16[2,256,256]{2,1,0:T(8,128)(2,1)S(1)} %pad_maximum_fusion.5.refs_8_), channel_id=1, source_target_pairs={{0,8},{8,16},{16,24},{24,0},{1,9},{9,17},{17,25},{25,1},{2,10},{10... | collective-permute-start | bytes 786440 | tf_op jit(solution)/shard_map/ppermute | solution.py:28
  122.1 19.2 %collective-permute-start.3 = (bf16[2,256,256]{2,1,0:T(8,128)(2,1)S(1)}, bf16[2,256,256]{2,1,0:T(8,128)(2,1)}, u32[]{:S(2)}, u32[]{:S(2)}) collective-permute-start(bf16[2,256,256]{2,1,0:T(8,128)(2,1)S(1)} %pad_maximum_fusion.3.refs_0_), channel_id=1, source_target_pairs={{0,32},{32,64},{64,96},{96,0},{1,33},{33,65},{65,97},{97,1},{2,34}... | collective-permute-start | bytes 786440 | tf_op jit(solution)/shard_map/ppermute | solution.py:28
  124.4 16.9 %collective-permute-start.17 = (bf16[2,256,256]{2,1,0:T(8,128)(2,1)S(1)}, bf16[2,256,256]{2,1,0:T(8,128)(2,1)S(1)}, u32[]{:S(2)}, u32[]{:S(2)}) collective-permute-start(bf16[2,256,256]{2,1,0:T(8,128)(2,1)S(1)} %pad_maximum_fusion.5.refs_8_), channel_id=1, source_target_pairs={{0,24},{8,0},{16,8},{24,16},{1,25},{9,1},{17,9},{25,17},{2,26},{10... | collective-permute-start | bytes 786440 | tf_op jit(solution)/shard_map/ppermute | solution.py:28
  132.3 14.2 %collective-permute-start.8 = (bf16[2,256,256]{2,1,0:T(8,128)(2,1)S(1)}, bf16[2,256,256]{2,1,0:T(8,128)(2,1)S(1)}, u32[]{:S(2)}, u32[]{:S(2)}) collective-permute-start(bf16[2,256,256]{2,1,0:T(8,128)(2,1)S(1)} %pad_maximum_fusion.3.refs_0_), channel_id=1, source_target_pairs={{0,96},{32,0},{64,32},{96,64},{1,97},{33,1},{65,33},{97,65},{2,98}... | collective-permute-start | bytes 786440 | tf_op jit(solution)/shard_map/ppermute | solution.py:28
  135.2 14.2 %collective-permute-start.16 = (bf16[2,256,256]{2,1,0:T(8,128)(2,1)}, bf16[2,256,256]{2,1,0:T(8,128)(2,1)}, u32[]{:S(2)}, u32[]{:S(2)}) collective-permute-start(bf16[2,256,256]{2,1,0:T(8,128)(2,1)} %collective-permute-done.15.refs_15_), channel_id=1, source_target_pairs={{0,24},{8,0},{16,8},{24,16},{1,25},{9,1},{17,9},{25,17},{2,26},{10... | collective-permute-start | bytes 786440 | tf_op jit(solution)/shard_map/ppermute | solution.py:28
  141.3 14.7 %collective-permute-start.7 = (bf16[2,256,256]{2,1,0:T(8,128)(2,1)}, bf16[2,256,256]{2,1,0:T(8,128)(2,1)}, u32[]{:S(2)}, u32[]{:S(2)}) collective-permute-start(bf16[2,256,256]{2,1,0:T(8,128)(2,1)} %collective-permute-done.6.refs_7_), channel_id=1, source_target_pairs={{0,96},{32,0},{64,32},{96,64},{1,97},{33,1},{65,33},{97,65},{2,98}... | collective-permute-start | bytes 786440 | tf_op jit(solution)/shard_map/ppermute | solution.py:28
  142.0 14.4 %collective-permute-start.14 = (bf16[2,256,256]{2,1,0:T(8,128)(2,1)}, bf16[2,256,256]{2,1,0:T(8,128)(2,1)}, u32[]{:S(2)}, u32[]{:S(2)}) collective-permute-start(bf16[2,256,256]{2,1,0:T(8,128)(2,1)} %collective-permute-done.12.refs_10_), channel_id=1, source_target_pairs={{0,8},{8,16},{16,24},{24,0},{1,9},{9,17},{17,25},{25,1},{2,10},{10... | collective-permute-start | bytes 786440 | tf_op jit(solution)/shard_map/ppermute | solution.py:28
  147.2 12.4 %collective-permute-start.5 = (bf16[2,256,256]{2,1,0:T(8,128)(2,1)}, bf16[2,256,256]{2,1,0:T(8,128)(2,1)}, u32[]{:S(2)}, u32[]{:S(2)}) collective-permute-start(bf16[2,256,256]{2,1,0:T(8,128)(2,1)} %collective-permute-done.3.refs_2_), channel_id=1, source_target_pairs={{0,32},{32,64},{64,96},{96,0},{1,33},{33,65},{65,97},{97,1},{2,34}... | collective-permute-start | bytes 786440 | tf_op jit(solution)/shard_map/ppermute | solution.py:28
  171.1 11.8 %collective-permute-start.21 = (f32[3,34,256]{2,1,0:T(8,128)S(1)}, f32[3,34,256]{2,1,0:T(8,128)S(1)}, u32[]{:S(2)}, u32[]{:S(2)}) collective-permute-start(f32[3,34,256]{2,1,0:T(8,128)S(1)} %pad_maximum_fusion.7.chan_own), channel_id=1, source_target_pairs={{0,1},{1,0},{2,3},{3,2},{4,5},{5,4},{6,7},{7,6},{8,9},{9,8},{10,11... | collective-permute-start | bytes 313352 | tf_op jit(solution)/shard_map/ppermute | solution.py:24
  172.4 10.6 %collective-permute-start.19 = (bf16[64,256]{1,0:T(8,128)(2,1)S(1)}, bf16[64,256]{1,0:T(8,128)(2,1)S(1)}, u32[]{:S(2)}, u32[]{:S(2)}) collective-permute-start(bf16[64,256]{1,0:T(8,128)(2,1)S(1)} %pad_maximum_fusion.8), channel_id=1, source_target_pairs={{0,1},{1,8},{8,9},{9,16},{16,17},{17,24},{24,25},{25,32},{32,33},{... | collective-permute-start | bytes 98312 | tf_op jit(solution)/shard_map/ppermute | solution.py:365
  185.6 8.5 %collective-permute-start.22 = (bf16[208,512]{1,0:T(8,128)(2,1)S(1)}, bf16[208,512]{1,0:T(8,128)(2,1)S(1)}, u32[]{:S(2)}, u32[]{:S(2)}) collective-permute-start(bf16[208,512]{1,0:T(8,128)(2,1)S(1)} %conv.3.refs_0_), channel_id=1, source_target_pairs={{0,2},{2,4},{4,6},{6,0},{1,3},{3,5},{5,7},{7,1},{8,10},{10,12},{12... | collective-permute-start | bytes 638984 | tf_op jit(solution)/shard_map/ppermute | solution.py:28
  187.7 11.8 %collective-permute-start.23 = (bf16[208,512]{1,0:T(8,128)(2,1)S(1)}, bf16[208,512]{1,0:T(8,128)(2,1)S(1)}, u32[]{:S(2)}, u32[]{:S(2)}) collective-permute-start(bf16[208,512]{1,0:T(8,128)(2,1)S(1)} %conv.3.refs_0_), channel_id=1, source_target_pairs={{0,4},{2,6},{4,0},{6,2},{1,5},{3,7},{5,1},{7,3},{8,12},{10,14},{12... | collective-permute-start | bytes 638984 | tf_op jit(solution)/shard_map/ppermute | solution.py:28
  190.4 9.1 %collective-permute-start.24 = (bf16[208,512]{1,0:T(8,128)(2,1)S(1)}, bf16[208,512]{1,0:T(8,128)(2,1)S(1)}, u32[]{:S(2)}, u32[]{:S(2)}) collective-permute-start(bf16[208,512]{1,0:T(8,128)(2,1)S(1)} %conv.3.refs_0_), channel_id=1, source_target_pairs={{0,6},{2,0},{4,2},{6,4},{1,7},{3,1},{5,3},{7,5},{8,14},{10,8},{12,... | collective-permute-start | bytes 638984 | tf_op jit(solution)/shard_map/ppermute | solution.py:28
  206.7 8.5 %collective-permute-start.26 = (bf16[192,512]{1,0:T(8,128)(2,1)S(1)}, bf16[192,512]{1,0:T(8,128)(2,1)S(1)}, u32[]{:S(2)}, u32[]{:S(2)}) collective-permute-start(bf16[192,512]{1,0:T(8,128)(2,1)S(1)} %get-tuple-element.32.refs_0_.refs_4_), channel_id=1, source_target_pairs={{0,2},{2,4},{4,6},{6,0},{1,3},{3,5},{5,7},{7,1},{8,10},{10,12},{12... | collective-permute-start | bytes 589832 | tf_op jit(solution)/shard_map/ppermute | solution.py:28
  210.0 9.4 %collective-permute-start.27 = (bf16[192,512]{1,0:T(8,128)(2,1)S(1)}, bf16[192,512]{1,0:T(8,128)(2,1)S(1)}, u32[]{:S(2)}, u32[]{:S(2)}) collective-permute-start(bf16[192,512]{1,0:T(8,128)(2,1)S(1)} %get-tuple-element.33.refs_1_.refs_5_), channel_id=1, source_target_pairs={{0,2},{2,4},{4,6},{6,0},{1,3},{3,5},{5,7},{7,1},{8,10},{10,12},{12... | collective-permute-start | bytes 589832 | tf_op jit(solution)/shard_map/ppermute | solution.py:28
  210.0 10.0 %collective-permute-start.31 = (bf16[192,512]{1,0:T(8,128)(2,1)S(1)}, bf16[192,512]{1,0:T(8,128)(2,1)S(1)}, u32[]{:S(2)}, u32[]{:S(2)}) collective-permute-start(bf16[192,512]{1,0:T(8,128)(2,1)S(1)} %get-tuple-element.32.refs_0_.refs_4_), channel_id=1, source_target_pairs={{0,6},{2,0},{4,2},{6,4},{1,7},{3,1},{5,3},{7,5},{8,14},{10,8},{12,... | collective-permute-start | bytes 589832 | tf_op jit(solution)/shard_map/ppermute | solution.py:28
  237.7 10.0 %collective-permute-start.35 = (bf16[208,512]{1,0:T(8,128)(2,1)S(1)}, bf16[208,512]{1,0:T(8,128)(2,1)S(1)}, u32[]{:S(2)}, u32[]{:S(2)}) collective-permute-start(bf16[208,512]{1,0:T(8,128)(2,1)S(1)} %conv.4.refs_0_), channel_id=1, source_target_pairs={{0,4},{2,6},{4,0},{6,2},{1,5},{3,7},{5,1},{7,3},{8,12},{10,14},{12... | collective-permute-start | bytes 638984 | tf_op jit(solution)/shard_map/ppermute | solution.py:28
  251.3 17.0 %collective-permute-start.43 = (bf16[16,384,512]{2,1,0:T(8,128)(2,1)}, bf16[16,384,512]{2,1,0:T(8,128)(2,1)S(1)}, u32[]{:S(2)}, u32[]{:S(2)}) collective-permute-start(bf16[16,384,512]{2,1,0:T(8,128)(2,1)} %bitcast.42), channel_id=1, source_target_pairs={{0,1},{1,0},{2,3},{3,2},{4,5},{5,4},{6,7},{7,6},{8,9},{9,8},{10,11... | collective-permute-start | bytes 18874376 | tf_op jit(solution)/shard_map/ppermute | solution.py:24
  251.4 9.1 %collective-permute-start.37 = (bf16[192,512]{1,0:T(8,128)(2,1)S(1)}, bf16[192,512]{1,0:T(8,128)(2,1)S(1)}, u32[]{:S(2)}, u32[]{:S(2)}) collective-permute-start(bf16[192,512]{1,0:T(8,128)(2,1)S(1)} %get-tuple-element.39.refs_0_.refs_4_), channel_id=1, source_target_pairs={{0,2},{2,4},{4,6},{6,0},{1,3},{3,5},{5,7},{7,1},{8,10},{10,12},{12... | collective-permute-start | bytes 589832 | tf_op jit(solution)/shard_map/ppermute | solution.py:28
  254.7 10.0 %collective-permute-start.38 = (bf16[192,512]{1,0:T(8,128)(2,1)S(1)}, bf16[192,512]{1,0:T(8,128)(2,1)S(1)}, u32[]{:S(2)}, u32[]{:S(2)}) collective-permute-start(bf16[192,512]{1,0:T(8,128)(2,1)S(1)} %get-tuple-element.40.refs_1_.refs_5_), channel_id=1, source_target_pairs={{0,2},{2,4},{4,6},{6,0},{1,3},{3,5},{5,7},{7,1},{8,10},{10,12},{12... | collective-permute-start | bytes 589832 | tf_op jit(solution)/shard_map/ppermute | solution.py:28
  254.9 10.0 %collective-permute-start.42 = (bf16[192,512]{1,0:T(8,128)(2,1)S(1)}, bf16[192,512]{1,0:T(8,128)(2,1)S(1)}, u32[]{:S(2)}, u32[]{:S(2)}) collective-permute-start(bf16[192,512]{1,0:T(8,128)(2,1)S(1)} %get-tuple-element.39.refs_0_.refs_4_), channel_id=1, source_target_pairs={{0,6},{2,0},{4,2},{6,4},{1,7},{3,1},{5,3},{7,5},{8,14},{10,8},{12,... | collective-permute-start | bytes 589832 | tf_op jit(solution)/shard_map/ppermute | solution.py:28
  285.7 10.0 %collective-permute-start.46 = (bf16[208,512]{1,0:T(8,128)(2,1)S(1)}, bf16[208,512]{1,0:T(8,128)(2,1)S(1)}, u32[]{:S(2)}, u32[]{:S(2)}) collective-permute-start(bf16[208,512]{1,0:T(8,128)(2,1)S(1)} %conv.5.refs_0_), channel_id=1, source_target_pairs={{0,4},{2,6},{4,0},{6,2},{1,5},{3,7},{5,1},{7,3},{8,12},{10,14},{12... | collective-permute-start | bytes 638984 | tf_op jit(solution)/shard_map/ppermute | solution.py:28
  (48 other events, 702.3 us)
Sparse Core Ops, SparseCore 0:
  10.6 72.7 all-gather.6
  85.5 76.5 all-gather.4
where the time goes:
time: 311 us; the launch traced here: 309 us
  waiting for transfers between devices  164 us (53%)
  starting transfers between devices  68.7 us (22%)
  Pallas kernels  33 us (11%)
  local copies, waits for them, and re-layouts  25 us (8%)
  between operations  13.8 us (4%)
  other arithmetic  4.51 us (1%)
    all_gather x2, waiting for transfers between devices, all_rows(): return lax.all_gather(jnp.concatenate(parts, axis=0), ('z', 'y'), axis=0)  72.1 us
    ppermute x39, waiting for transfers between devices, shift(): return lax.ppermute(a, axis, [(i, (i + by) % 4) for i in range(4)])  68.8 us
    ppermute x39, starting transfers between devices, shift(): return lax.ppermute(a, axis, [(i, (i + by) % 4) for i in range(4)])  55.5 us
    unnamed x56, local copies, waits for them, and re-layouts  17.9 us
    pallas_call x3, Pallas kernels, mix_call(): pl.pallas_call(functools.partial(mix_kernel, at), in_specs=[SMEM] + [VMEM...  11.2 us
    ppermute x3, waiting for transfers between devices, layers(): edge = lax.ppermute(edge, ('z', 'y', 'c'), onward)  10.8 us
    pallas_call x2, Pallas kernels, glu_call(): pl.pallas_call(functools.partial(glu_kernel, at), in_specs=[SMEM] + [VMEM...  8.35 us
    pallas_call x3, Pallas kernels, conv_call(): pl.pallas_call(functools.partial(conv_kernel, l), out_shape=jax.ShapeDtyp...  8.04 us
  transfers between devices with their start and end apart: 52, of which 35 were waited for; matrix products, arithmetic and copies ran while one was open for 2% of the time, Pallas kernels for 7%

commit v1 on v0

--- a/solution.py
+++ b/solution.py
@@ -20,6 +20,10 @@
 HBM = pl.BlockSpec(memory_space=pltpu.HBM)
 
 
+def in_hbm(a):
+    return pltpu.with_memory_space_constraint(a, pltpu.HBM)
+
+
 def swap(a):
     return lax.ppermute(a, "c", [(0, 1), (1, 0)])
 
@@ -38,10 +42,6 @@
     a, b, left_a, left_b, right_a, right_b = halves
     two = shift(left_a, 1, axis), shift(right_b, 3, axis)
     return a, b, left_a, left_b, *two, right_a, right_b
-
-
-def ring(a, b, axis="x"):
-    return far(near(a, b, axis), axis)
 
 
 def around(a, axis="x"):
@@ -191,7 +191,7 @@
         ),
         compiler_params=pltpu.CompilerParams(vmem_limit_bytes=16 * 2**20),
         name="glu",
-    )(ix, *xp, gain.reshape(8, 1, 512), w_own, w_oth)
+    )(ix, *xp, gain.reshape(8, 1, 512), in_hbm(w_own), w_oth)
 
 
 def thirds(v):
@@ -254,13 +254,16 @@
 
 def mix_kernel(at, ix, *refs):
     cp, state, refs = refs[:4], refs[4:6], refs[6:]
-    weights, outs, (mixed, buf, sem) = refs[:2], refs[2:4], refs[4:]
+    weights, outs, (mixed, buf, old, sem, sem2) = refs[:2], refs[2:4], refs[4:]
     x, c = ix[0], ix[3]
     copies = [
         fetch(w, (x - d) & 3, 128, at[h], buf.at[h, n], sem.at[h, n])
         for n, d in enumerate(ARRIVAL)
         for h, w in enumerate(weights)
     ]
+    olds = [pltpu.make_async_copy(state[h], old.at[h], sem2.at[h]) for h in range(2)]
+    for copy in olds:
+        copy.start()
     lane = lax.broadcasted_iota(jnp.int32, (64, 128), 1)
     row = lax.broadcasted_iota(jnp.int32, (64, 128), 0)
 
@@ -301,18 +304,21 @@
             copies[2 * n + h].wait()
             acc[h] = acc[h] + dot(mixed[d], in_order(buf.at[h, n], c))
     for h in range(2):
-        outs[h][...] = (state[h][...].astype(F32) + acc[h]).astype(BF16)
+        olds[h].wait()
+        outs[h][...] = (old[h].astype(F32) + acc[h]).astype(BF16)
 
 
 def mix_call(ix, cp, state, weights, at):
     return pl.pallas_call(
         functools.partial(mix_kernel, at),
-        in_specs=[SMEM] + [VMEM] * 6 + [HBM] * 2,
+        in_specs=[SMEM] + [VMEM] * 4 + [HBM] * 4,
         out_specs=[VMEM] * 2,
         scratch_shapes=[
             pltpu.VMEM((4, T, 512), BF16),
             pltpu.VMEM((2, 4, 4, 128, 512), BF16),
+            pltpu.VMEM((2, T, 512), BF16),
             pltpu.SemaphoreType.DMA((2, 4)),
+            pltpu.SemaphoreType.DMA((2,)),
         ],
         out_shape=[jax.ShapeDtypeStruct((T, 512), BF16)] * 2,
         cost_estimate=pl.CostEstimate(
@@ -320,7 +326,7 @@
         ),
         compiler_params=pltpu.CompilerParams(vmem_limit_bytes=12 * 2**20),
         name="mix",
-    )(ix, *cp, *state, *weights)
+    )(ix, *cp, *state, in_hbm(weights[0]), weights[1])
 
 
 def layers(
@@ -332,10 +338,12 @@
     def pair(l):
         return jnp.concatenate([w_value[l], w_gate[l]], axis=1)
 
-    def all_rows(*parts):
-        return lax.all_gather(jnp.concatenate(parts, axis=0), ("z", "y"), axis=0)
-
-    middle = all_rows(pair(1), w_out[0], w_out[1])
+    def all_rows(part):
+        return lax.all_gather(part, ("z", "y"), axis=0)
+
+    packed = jnp.concatenate([pair(1), w_out[0], w_out[1]], axis=0)
+    packed, hidden = lax.optimization_barrier((packed, hidden))
+    middle = all_rows(packed)
     blocks = jnp.moveaxis(hidden.reshape(2 * T, 2, 256), 1, 0)
     first = to_all(blocks, ("x", "c")).reshape(16, 2 * T, 256)
 
@@ -361,7 +369,9 @@
             edge = jnp.concatenate([own[-HALO:], oth[-HALO:]], axis=0)
         else:
             weights = weights if l == 1 else last
-            own, oth, edge = glu_call(ix, ring(*state), norm_gain[l], *weights, 0)
+            halves = near(*state, "x")
+            blocks = far(halves, "x")
+            own, oth, edge = glu_call(ix, blocks, norm_gain[l], *weights, 0)
         edge = lax.ppermute(edge, ("z", "y", "c"), onward)
         dev = conv_call(l, edge, own, oth, lim, *chan)
         if l == 0:
@@ -369,11 +379,11 @@
             part = swap(part)
             middle, part = lax.optimization_barrier((middle, part))
             weights = (middle, swap(middle))
+            state = [in_hbm(v) for v in state]
         devs = around(dev)
         with_out = ((middle, part), (2, 0)) if l == 0 else (weights, (4 - l, 4 - l))
         state = mix_call(ix, devs, state, *with_out)
         if l == 1:
-            last, *state = lax.optimization_barrier((last, *state))
             last = (last, swap(last))
 
     own, oth = state[0], swap(state[1])

time: 311 us -> 354 us (1.14)
  waiting for transfers between devices: 164 us -> 204 us
  starting transfers between devices: 68.7 us -> 74.5 us
    all_gather x2, waiting for transfers between devices: 72.1 us -> 128 us  [all_rows(): return lax.all_gather(part, ('z', 'y'), axis=0)]
    ppermute x39, waiting for transfers between devices: 68.8 us -> 53.5 us  [shift(): return lax.ppermute(a, axis, [(i, (i + by) % 4) for i in range(4)])]
    ppermute x39, starting transfers between devices: 55.5 us -> 60.6 us  [shift(): return lax.ppermute(a, axis, [(i, (i + by) % 4) for i in range(4)])]
    unnamed x56 -> x58, local copies, waits for them, and re-layouts: 17.9 us -> 14.9 us
  transfers between devices with their start and end apart: 52 -> 52, of which waited for: 35 -> 31; matrix products, arithmetic and copies ran while one was open for 2% -> 2% of each run, Pallas kernels for 7% -> 6%
where the time goes in v1:
time: 354 us; the launch traced here: 353 us
  waiting for transfers between devices  204 us (58%)
  starting transfers between devices  74.5 us (21%)
  Pallas kernels  33.8 us (10%)
  local copies, waits for them, and re-layouts  22 us (6%)
  between operations  13.8 us (4%)
  other arithmetic  4.52 us (1%)
    all_gather x2, waiting for transfers between devices, all_rows(): return lax.all_gather(part, ('z', 'y'), axis=0)  128 us
    ppermute x39, starting transfers between devices, shift(): return lax.ppermute(a, axis, [(i, (i + by) % 4) for i in range(4)])  60.6 us
    ppermute x39, waiting for transfers between devices, shift(): return lax.ppermute(a, axis, [(i, (i + by) % 4) for i in range(4)])  53.5 us
    unnamed x58, local copies, waits for them, and re-layouts  14.9 us
    pallas_call x3, Pallas kernels, mix_call(): pl.pallas_call(functools.partial(mix_kernel, at), in_specs=[SMEM] + [VMEM...  11.8 us
    ppermute x3, waiting for transfers between devices, layers(): edge = lax.ppermute(edge, ('z', 'y', 'c'), onward)  10.8 us
    pallas_call x2, Pallas kernels, glu_call(): pl.pallas_call(functools.partial(glu_kernel, at), in_specs=[SMEM] + [VMEM...  9.61 us
    pallas_call x3, Pallas kernels, conv_call(): pl.pallas_call(functools.partial(conv_kernel, l), out_shape=jax.ShapeDtyp...  7.3 us
  transfers between devices with their start and end apart: 52, of which 31 were waited for; matrix products, arithmetic and copies ran while one was open for 2% of the time, Pallas kernels for 6%

profile of v1, /device:TPU:32, one launch (start us, length us, event | category | flops | bytes accessed | tf_op | source)
XLA Modules:
  0.0 352.5 jit_solution(10331648655648464295)
XLA Ops:
  11.4 72.1 %all-gather.5.cloned.1.call-done = bf16[8192,512]{1,0:T(8,128)(2,1)} async-done(((bf16[512,512]{1,0:T(8,128)(2,1)}), bf16[8192,512]{1,0:T(8,128)(2,1)}) %all-gather.5.cloned.1.call-update) | async-done | bytes 8388624 | tf_op jit(solution)/shard_map/all_gather | solution.py:342
  85.3 4.1 %collective-permute-done.25.refs_7_ = bf16[16,128,512]{2,1,0:T(8,128)(2,1)S(1)} collective-permute-done((bf16[16,128,512]{2,1,0:T(8,128)(2,1)S(1)}, bf16[16,128,512]{2,1,0:T(8,128)(2,1)S(1)}, u32[]{:S(2)}, u32[]{:S(2)}) %collective-permute-start.25) | collective-permute-done | bytes 2097184 | tf_op jit(solution)/shard_map/ppermute | solution.py:28
  90.9 55.7 %all-gather.7.cloned.1.call-done = bf16[6144,512]{1,0:T(8,128)(2,1)} async-done(((bf16[384,512]{1,0:T(8,128)(2,1)}), bf16[6144,512]{1,0:T(8,128)(2,1)}) %all-gather.7.cloned.1.call-update) | async-done | bytes 6291472 | tf_op jit(solution)/shard_map/all_gather | solution.py:342
  148.7 4.4 %all-to-all-start = ((bf16[8,2,384,256]{3,2,1,0:T(8,128)(2,1)}), bf16[8,2,384,256]{3,2,1,0:T(8,128)(2,1)S(1)}, u32[]{:S(2)}, u32[]{:S(2)}) async-start(bf16[8,2,384,256]{3,2,1,0:T(8,128)(2,1)} %broadcast_in_dim.15), calls=%async_computation | async-start | bytes 6291456 | tf_op jit(solution)/shard_map/all_to_all | solution.py:54
  158.3 3.0 collective-permute-done.10
  166.4 2.8 collective-permute-start.15
  179.8 3.3 collective-permute-start.3
  186.0 2.9 collective-permute-start.8
  193.3 3.0 collective-permute-start.7
  200.5 4.8 %collective-permute-done.14.refs_12_ = bf16[2,256,256]{2,1,0:T(8,128)(2,1)} collective-permute-done((bf16[2,256,256]{2,1,0:T(8,128)(2,1)}, bf16[2,256,256]{2,1,0:T(8,128)(2,1)}, u32[]{:S(2)}, u32[]{:S(2)}) %collective-permute-start.14) | collective-permute-done | bytes 262176 | tf_op jit(solution)/shard_map/ppermute | solution.py:32
  214.1 4.2 %glu0.1 = (bf16[192,256]{1,0:T(8,128)(2,1)S(1)}, bf16[192,256]{1,0:T(8,128)(2,1)S(1)}, bf16[192,512]{1,0:T(8,128)(2,1)S(1)}, bf16[192,512]{1,0:T(8,128)(2,1)S(1)}) custom-call(s32[4]{0:T(128)S(1)} %pad_add_fusion.ix, bf16[16,384,256]{2,1,0:T(8,128)(2,1)S(1)} %bitcast.35, f32[16,1,256]{2,1,0:T(1,128)S(1)} %bitcast.38, bf16[2,256,256]{2,1,0:T(8,128)(2,1)S(1)} %copy-done.7, ...), custom_call_target="tpu_custom_call" | custom-call | flops 1610612736 | bytes 8388608 | tf_op jit(solution)/shard_map/glu0/pallas_call | solution.py:96
  224.4 5.7 %collective-permute-done.20 = s32[384]{0:T(512)S(1)} collective-permute-done((s32[384]{0:T(512)S(1)}, s32[384]{0:T(512)S(1)}, u32[]{:S(2)}, u32[]{:S(2)}) %collective-permute-start.20) | collective-permute-done | bytes 1568 | tf_op jit(solution)/shard_map/ppermute | solution.py:356
  234.5 2.7 collective-permute-start.23
  238.7 3.6 %collective-permute-done.22.refs_1_ = bf16[208,512]{1,0:T(8,128)(2,1)S(1)} collective-permute-done((bf16[208,512]{1,0:T(8,128)(2,1)S(1)}, bf16[208,512]{1,0:T(8,128)(2,1)S(1)}, u32[]{:S(2)}, u32[]{:S(2)}) %collective-permute-start.22) | collective-permute-done | bytes 213024 | tf_op jit(solution)/shard_map/ppermute | solution.py:32
  242.3 3.8 %collective-permute-done.23.refs_2_ = bf16[208,512]{1,0:T(8,128)(2,1)S(1)} collective-permute-done((bf16[208,512]{1,0:T(8,128)(2,1)S(1)}, bf16[208,512]{1,0:T(8,128)(2,1)S(1)}, u32[]{:S(2)}, u32[]{:S(2)}) %collective-permute-start.23) | collective-permute-done | bytes 213024 | tf_op jit(solution)/shard_map/ppermute | solution.py:32
  246.1 3.7 %mix.3 = (bf16[192,512]{1,0:T(8,128)(2,1)S(1)}, bf16[192,512]{1,0:T(8,128)(2,1)S(1)}) custom-call(s32[4]{0:T(128)S(1)} %pad_add_fusion.ix, bf16[208,512]{1,0:T(8,128)(2,1)S(1)} %conv.3.refs_0_, bf16[208,512]{1,0:T(8,128)(2,1)S(1)} %collective-permute-done.22.refs_1_, bf16[208,512]{1,0:T(8,128)(2,1)S(1)} %collective-permute-done.23.refs_2_, ...), custom_call_target="tpu_custom_call" | custom-call | flops 805306368 | bytes 6291456 | tf_op jit(solution)/shard_map/mix/pallas_call | solution.py:312
  253.7 4.9 %collective-permute-done.26.refs_2_ = bf16[192,512]{1,0:T(8,128)(2,1)S(1)} collective-permute-done((bf16[192,512]{1,0:T(8,128)(2,1)S(1)}, bf16[192,512]{1,0:T(8,128)(2,1)S(1)}, u32[]{:S(2)}, u32[]{:S(2)}) %collective-permute-start.26) | collective-permute-done | bytes 196640 | tf_op jit(solution)/shard_map/ppermute | solution.py:32
  261.6 2.9 collective-permute-start.30
  268.4 4.8 %glu.2 = (bf16[192,256]{1,0:T(8,128)(2,1)S(1)}, bf16[192,256]{1,0:T(8,128)(2,1)S(1)}, bf16[64,256]{1,0:T(8,128)(2,1)S(1)}) custom-call(s32[4]{0:T(128)S(1)} %pad_add_fusion.ix, bf16[192,512]{1,0:T(8,128)(2,1)S(1)} %get-tuple-element.33.refs_0_.refs_4_, bf16[192,512]{1,0:T(8,128)(2,1)S(1)} %get-tuple-element.34.refs_1_.refs_5_, ...), custom_call_target="tpu_custom_call" | custom-call | flops 1610612736 | bytes 10485760 | tf_op jit(solution)/shard_map/glu/pallas_call | solution.py:176
  275.2 5.4 %collective-permute-done.33.edge = bf16[64,256]{1,0:T(8,128)(2,1)S(1)} collective-permute-done((bf16[64,256]{1,0:T(8,128)(2,1)S(1)}, bf16[64,256]{1,0:T(8,128)(2,1)S(1)}, u32[]{:S(2)}, u32[]{:S(2)}) %collective-permute-start.33) | collective-permute-done | bytes 32800 | tf_op jit(solution)/shard_map/ppermute | solution.py:375
  284.0 3.6 %collective-permute-start.35 = (bf16[208,512]{1,0:T(8,128)(2,1)S(1)}, bf16[208,512]{1,0:T(8,128)(2,1)S(1)}, u32[]{:S(2)}, u32[]{:S(2)}) collective-permute-start(bf16[208,512]{1,0:T(8,128)(2,1)S(1)} %conv.4.refs_0_), channel_id=1, source_target_pairs={{0,4},{2,6},{4,0},{6,2},{1,5},{3,7},{5,1},{7,3},{8,12},{10,14},{12... | collective-permute-start | bytes 638984 | tf_op jit(solution)/shard_map/ppermute | solution.py:32
  287.6 4.1 %collective-permute-done.34.refs_1_ = bf16[208,512]{1,0:T(8,128)(2,1)S(1)} collective-permute-done((bf16[208,512]{1,0:T(8,128)(2,1)S(1)}, bf16[208,512]{1,0:T(8,128)(2,1)S(1)}, u32[]{:S(2)}, u32[]{:S(2)}) %collective-permute-start.34) | collective-permute-done | bytes 213024 | tf_op jit(solution)/shard_map/ppermute | solution.py:32
  294.0 4.1 %mix.4 = (bf16[192,512]{1,0:T(8,128)(2,1)S(1)}, bf16[192,512]{1,0:T(8,128)(2,1)S(1)}) custom-call(s32[4]{0:T(128)S(1)} %pad_add_fusion.ix, bf16[208,512]{1,0:T(8,128)(2,1)S(1)} %conv.4.refs_0_, bf16[208,512]{1,0:T(8,128)(2,1)S(1)} %collective-permute-done.34.refs_1_, bf16[208,512]{1,0:T(8,128)(2,1)S(1)} %collective-permute-done.35.refs_2_, ...), custom_call_target="tpu_custom_call" | custom-call | flops 805306368 | bytes 6291456 | tf_op jit(solution)/shard_map/mix/pallas_call | solution.py:312
  298.6 2.8 collective-permute-start.40
  301.4 3.2 collective-permute-start.42
  306.7 3.5 collective-permute-start.41
  310.2 3.4 collective-permute-done.39.refs_4_
  313.5 4.8 %glu.3 = (bf16[192,256]{1,0:T(8,128)(2,1)S(1)}, bf16[192,256]{1,0:T(8,128)(2,1)S(1)}, bf16[64,256]{1,0:T(8,128)(2,1)S(1)}) custom-call(s32[4]{0:T(128)S(1)} %pad_add_fusion.ix, bf16[192,512]{1,0:T(8,128)(2,1)S(1)} %get-tuple-element.38.refs_0_.refs_4_, bf16[192,512]{1,0:T(8,128)(2,1)S(1)} %get-tuple-element.39.refs_1_.refs_5_, ...), custom_call_target="tpu_custom_call" | custom-call | flops 1610612736 | bytes 10485760 | tf_op jit(solution)/shard_map/glu/pallas_call | solution.py:176
  320.3 5.4 %collective-permute-done.44.edge = bf16[64,256]{1,0:T(8,128)(2,1)S(1)} collective-permute-done((bf16[64,256]{1,0:T(8,128)(2,1)S(1)}, bf16[64,256]{1,0:T(8,128)(2,1)S(1)}, u32[]{:S(2)}, u32[]{:S(2)}) %collective-permute-start.44) | collective-permute-done | bytes 32800 | tf_op jit(solution)/shard_map/ppermute | solution.py:375
  328.2 5.0 %collective-permute-start.46 = (bf16[208,512]{1,0:T(8,128)(2,1)S(1)}, bf16[208,512]{1,0:T(8,128)(2,1)S(1)}, u32[]{:S(2)}, u32[]{:S(2)}) collective-permute-start(bf16[208,512]{1,0:T(8,128)(2,1)S(1)} %conv.5.refs_0_), channel_id=1, source_target_pairs={{0,4},{2,6},{4,0},{6,2},{1,5},{3,7},{5,1},{7,3},{8,12},{10,14},{12... | collective-permute-start | bytes 638984 | tf_op jit(solution)/shard_map/ppermute | solution.py:32
  333.2 3.6 %collective-permute-done.45.refs_1_ = bf16[208,512]{1,0:T(8,128)(2,1)S(1)} collective-permute-done((bf16[208,512]{1,0:T(8,128)(2,1)S(1)}, bf16[208,512]{1,0:T(8,128)(2,1)S(1)}, u32[]{:S(2)}, u32[]{:S(2)}) %collective-permute-start.45) | collective-permute-done | bytes 213024 | tf_op jit(solution)/shard_map/ppermute | solution.py:32
  339.3 4.1 %mix.5 = (bf16[192,512]{1,0:T(8,128)(2,1)S(1)}, bf16[192,512]{1,0:T(8,128)(2,1)S(1)}) custom-call(s32[4]{0:T(128)S(1)} %pad_add_fusion.ix, bf16[208,512]{1,0:T(8,128)(2,1)S(1)} %conv.5.refs_0_, bf16[208,512]{1,0:T(8,128)(2,1)S(1)} %collective-permute-done.45.refs_1_, bf16[208,512]{1,0:T(8,128)(2,1)S(1)} %collective-permute-done.46.refs_2_, ...), custom_call_target="tpu_custom_call" | custom-call | flops 805306368 | bytes 6291456 | tf_op jit(solution)/shard_map/mix/pallas_call | solution.py:312
  (167 shorter events, 93.5 us)
Async XLA Ops:
  6.5 76.9 %all-gather.5.cloned.1.call-start = ((), (), s32[]{:S(2)}) async-start(), calls=%async_computation.1 | async-start | bytes 8912896 | tf_op jit(solution)/shard_map/all_gather | solution.py:342
  10.5 136.0 %all-gather.7.cloned.1.call-start = ((), (), s32[]{:S(2)}) async-start(), calls=%async_computation.2 | async-start | bytes 6684672 | tf_op jit(solution)/shard_map/all_gather | solution.py:342
  90.7 177.7 %collective-permute-start.32 = (bf16[16,512,512]{2,1,0:T(8,128)(2,1)}, bf16[16,512,512]{2,1,0:T(8,128)(2,1)}, u32[]{:S(2)}, u32[]{:S(2)}) collective-permute-start(bf16[16,512,512]{2,1,0:T(8,128)(2,1)} %bitcast.40), channel_id=1, source_target_pairs={{0,1},{1,0},{2,3},{3,2},{4,5},{5,4},{6,7},{7,6},{8,9},{9,8},{10,11... | collective-permute-start | bytes 25165832 | tf_op jit(solution)/shard_map/ppermute | solution.py:28
  146.6 163.6 %collective-permute-start.43 = (bf16[16,384,512]{2,1,0:T(8,128)(2,1)}, bf16[16,384,512]{2,1,0:T(8,128)(2,1)}, u32[]{:S(2)}, u32[]{:S(2)}) collective-permute-start(bf16[16,384,512]{2,1,0:T(8,128)(2,1)} %bitcast.44), channel_id=1, source_target_pairs={{0,1},{1,0},{2,3},{3,2},{4,5},{5,4},{6,7},{7,6},{8,9},{9,8},{10,11... | collective-permute-start | bytes 18874376 | tf_op jit(solution)/shard_map/ppermute | solution.py:28
  148.7 56.7 %all-to-all-start = ((bf16[8,2,384,256]{3,2,1,0:T(8,128)(2,1)}), bf16[8,2,384,256]{3,2,1,0:T(8,128)(2,1)S(1)}, u32[]{:S(2)}, u32[]{:S(2)}) async-start(bf16[8,2,384,256]{3,2,1,0:T(8,128)(2,1)} %broadcast_in_dim.15), calls=%async_computation | async-start | bytes 6291456 | tf_op jit(solution)/shard_map/all_to_all | solution.py:54
  153.1 8.2 %collective-permute-start.10 = (bf16[256,256]{1,0:T(8,128)(2,1)}, bf16[256,256]{1,0:T(8,128)(2,1)S(1)}, u32[]{:S(2)}, u32[]{:S(2)}) collective-permute-start(bf16[256,256]{1,0:T(8,128)(2,1)} %get-tuple-element.52), channel_id=1, source_target_pairs={{0,64},{32,96},{64,0},{96,32},{1,65},{33,97},{65,1},{97,33},{2,66}... | collective-permute-start | bytes 393224 | tf_op jit(solution)/shard_map/ppermute | solution.py:32
  155.4 8.1 %collective-permute-start.11 = (bf16[256,256]{1,0:T(8,128)(2,1)}, bf16[256,256]{1,0:T(8,128)(2,1)S(1)}, u32[]{:S(2)}, u32[]{:S(2)}) collective-permute-start(bf16[256,256]{1,0:T(8,128)(2,1)} %get-tuple-element.52), channel_id=1, source_target_pairs={{0,96},{32,0},{64,32},{96,64},{1,97},{33,1},{65,33},{97,65},{2,98}... | collective-permute-start | bytes 393224 | tf_op jit(solution)/shard_map/ppermute | solution.py:32
  170.8 8.3 %collective-permute-start.13 = (bf16[2,256,256]{2,1,0:T(8,128)(2,1)S(1)}, bf16[2,256,256]{2,1,0:T(8,128)(2,1)S(1)}, u32[]{:S(2)}, u32[]{:S(2)}) collective-permute-start(bf16[2,256,256]{2,1,0:T(8,128)(2,1)S(1)} %pad_maximum_fusion.6.refs_9_), channel_id=1, source_target_pairs={{0,8},{8,16},{16,24},{24,0},{1,9},{9,17},{17,25},{25,1},{2,10},{10... | collective-permute-start | bytes 786440 | tf_op jit(solution)/shard_map/ppermute | solution.py:32
  173.1 10.0 %collective-permute-start.4 = (bf16[2,256,256]{2,1,0:T(8,128)(2,1)S(1)}, bf16[2,256,256]{2,1,0:T(8,128)(2,1)S(1)}, u32[]{:S(2)}, u32[]{:S(2)}) collective-permute-start(bf16[2,256,256]{2,1,0:T(8,128)(2,1)S(1)} %pad_maximum_fusion.4.refs_1_), channel_id=1, source_target_pairs={{0,32},{32,64},{64,96},{96,0},{1,33},{33,65},{65,97},{97,1},{2,34}... | collective-permute-start | bytes 786440 | tf_op jit(solution)/shard_map/ppermute | solution.py:32
  176.6 9.4 %collective-permute-start.12 = (bf16[2,256,256]{2,1,0:T(8,128)(2,1)S(1)}, bf16[2,256,256]{2,1,0:T(8,128)(2,1)}, u32[]{:S(2)}, u32[]{:S(2)}) collective-permute-start(bf16[2,256,256]{2,1,0:T(8,128)(2,1)S(1)} %pad_maximum_fusion.5.refs_8_), channel_id=1, source_target_pairs={{0,8},{8,16},{16,24},{24,0},{1,9},{9,17},{17,25},{25,1},{2,10},{10... | collective-permute-start | bytes 786440 | tf_op jit(solution)/shard_map/ppermute | solution.py:32
  179.8 9.8 %collective-permute-start.3 = (bf16[2,256,256]{2,1,0:T(8,128)(2,1)S(1)}, bf16[2,256,256]{2,1,0:T(8,128)(2,1)}, u32[]{:S(2)}, u32[]{:S(2)}) collective-permute-start(bf16[2,256,256]{2,1,0:T(8,128)(2,1)S(1)} %pad_maximum_fusion.3.refs_0_), channel_id=1, source_target_pairs={{0,32},{32,64},{64,96},{96,0},{1,33},{33,65},{65,97},{97,1},{2,34}... | collective-permute-start | bytes 786440 | tf_op jit(solution)/shard_map/ppermute | solution.py:32
  183.8 8.8 %collective-permute-start.17 = (bf16[2,256,256]{2,1,0:T(8,128)(2,1)S(1)}, bf16[2,256,256]{2,1,0:T(8,128)(2,1)S(1)}, u32[]{:S(2)}, u32[]{:S(2)}) collective-permute-start(bf16[2,256,256]{2,1,0:T(8,128)(2,1)S(1)} %pad_maximum_fusion.5.refs_8_), channel_id=1, source_target_pairs={{0,24},{8,0},{16,8},{24,16},{1,25},{9,1},{17,9},{25,17},{2,26},{10... | collective-permute-start | bytes 786440 | tf_op jit(solution)/shard_map/ppermute | solution.py:32
  186.0 10.3 %collective-permute-start.8 = (bf16[2,256,256]{2,1,0:T(8,128)(2,1)S(1)}, bf16[2,256,256]{2,1,0:T(8,128)(2,1)S(1)}, u32[]{:S(2)}, u32[]{:S(2)}) collective-permute-start(bf16[2,256,256]{2,1,0:T(8,128)(2,1)S(1)} %pad_maximum_fusion.3.refs_0_), channel_id=1, source_target_pairs={{0,96},{32,0},{64,32},{96,64},{1,97},{33,1},{65,33},{97,65},{2,98}... | collective-permute-start | bytes 786440 | tf_op jit(solution)/shard_map/ppermute | solution.py:32
  197.0 8.4 %collective-permute-start.14 = (bf16[2,256,256]{2,1,0:T(8,128)(2,1)}, bf16[2,256,256]{2,1,0:T(8,128)(2,1)}, u32[]{:S(2)}, u32[]{:S(2)}) collective-permute-start(bf16[2,256,256]{2,1,0:T(8,128)(2,1)} %collective-permute-done.12.refs_10_), channel_id=1, source_target_pairs={{0,8},{8,16},{16,24},{24,0},{1,9},{9,17},{17,25},{25,1},{2,10},{10... | collective-permute-start | bytes 786440 | tf_op jit(solution)/shard_map/ppermute | solution.py:32
  197.7 7.7 %collective-permute-start.5 = (bf16[2,256,256]{2,1,0:T(8,128)(2,1)}, bf16[2,256,256]{2,1,0:T(8,128)(2,1)}, u32[]{:S(2)}, u32[]{:S(2)}) collective-permute-start(bf16[2,256,256]{2,1,0:T(8,128)(2,1)} %collective-permute-done.3.refs_2_), channel_id=1, source_target_pairs={{0,32},{32,64},{64,96},{96,0},{1,33},{33,65},{65,97},{97,1},{2,34}... | collective-permute-start | bytes 786440 | tf_op jit(solution)/shard_map/ppermute | solution.py:32
  218.5 12.4 %collective-permute-start.21 = (f32[3,34,256]{2,1,0:T(8,128)S(1)}, f32[3,34,256]{2,1,0:T(8,128)S(1)}, u32[]{:S(2)}, u32[]{:S(2)}) collective-permute-start(f32[3,34,256]{2,1,0:T(8,128)S(1)} %pad_maximum_fusion.7.chan_own), channel_id=1, source_target_pairs={{0,1},{1,0},{2,3},{3,2},{4,5},{5,4},{6,7},{7,6},{8,9},{9,8},{10,11... | collective-permute-start | bytes 313352 | tf_op jit(solution)/shard_map/ppermute | solution.py:28
  219.8 11.2 %collective-permute-start.19 = (bf16[64,256]{1,0:T(8,128)(2,1)S(1)}, bf16[64,256]{1,0:T(8,128)(2,1)S(1)}, u32[]{:S(2)}, u32[]{:S(2)}) collective-permute-start(bf16[64,256]{1,0:T(8,128)(2,1)S(1)} %pad_maximum_fusion.8), channel_id=1, source_target_pairs={{0,1},{1,8},{8,9},{9,16},{16,17},{17,24},{24,25},{25,32},{32,33},{... | collective-permute-start | bytes 98312 | tf_op jit(solution)/shard_map/ppermute | solution.py:375
  221.8 8.3 %collective-permute-start.20 = (s32[384]{0:T(512)S(1)}, s32[384]{0:T(512)S(1)}, u32[]{:S(2)}, u32[]{:S(2)}) collective-permute-start(s32[384]{0:T(512)S(1)} %copy-done.28), channel_id=1, source_target_pairs={{0,8},{8,16},{16,24},{24,32},{32,40},{40,48},{48,56},{56,64},{64,7... | collective-permute-start | bytes 4616 | tf_op jit(solution)/shard_map/ppermute | solution.py:356
  233.4 8.9 %collective-permute-start.22 = (bf16[208,512]{1,0:T(8,128)(2,1)S(1)}, bf16[208,512]{1,0:T(8,128)(2,1)S(1)}, u32[]{:S(2)}, u32[]{:S(2)}) collective-permute-start(bf16[208,512]{1,0:T(8,128)(2,1)S(1)} %conv.3.refs_0_), channel_id=1, source_target_pairs={{0,2},{2,4},{4,6},{6,0},{1,3},{3,5},{5,7},{7,1},{8,10},{10,12},{12... | collective-permute-start | bytes 638984 | tf_op jit(solution)/shard_map/ppermute | solution.py:32
  234.5 11.5 %collective-permute-start.23 = (bf16[208,512]{1,0:T(8,128)(2,1)S(1)}, bf16[208,512]{1,0:T(8,128)(2,1)S(1)}, u32[]{:S(2)}, u32[]{:S(2)}) collective-permute-start(bf16[208,512]{1,0:T(8,128)(2,1)S(1)} %conv.3.refs_0_), channel_id=1, source_target_pairs={{0,4},{2,6},{4,0},{6,2},{1,5},{3,7},{5,1},{7,3},{8,12},{10,14},{12... | collective-permute-start | bytes 638984 | tf_op jit(solution)/shard_map/ppermute | solution.py:32
  237.2 8.9 %collective-permute-start.24 = (bf16[208,512]{1,0:T(8,128)(2,1)S(1)}, bf16[208,512]{1,0:T(8,128)(2,1)S(1)}, u32[]{:S(2)}, u32[]{:S(2)}) collective-permute-start(bf16[208,512]{1,0:T(8,128)(2,1)S(1)} %conv.3.refs_0_), channel_id=1, source_target_pairs={{0,6},{2,0},{4,2},{6,4},{1,7},{3,1},{5,3},{7,5},{8,14},{10,8},{12,... | collective-permute-start | bytes 638984 | tf_op jit(solution)/shard_map/ppermute | solution.py:32
  249.8 8.7 %collective-permute-start.26 = (bf16[192,512]{1,0:T(8,128)(2,1)S(1)}, bf16[192,512]{1,0:T(8,128)(2,1)S(1)}, u32[]{:S(2)}, u32[]{:S(2)}) collective-permute-start(bf16[192,512]{1,0:T(8,128)(2,1)S(1)} %get-tuple-element.33.refs_0_.refs_4_), channel_id=1, source_target_pairs={{0,2},{2,4},{4,6},{6,0},{1,3},{3,5},{5,7},{7,1},{8,10},{10,12},{12... | collective-permute-start | bytes 589832 | tf_op jit(solution)/shard_map/ppermute | solution.py:32
  251.6 8.7 %collective-permute-start.29 = (bf16[192,512]{1,0:T(8,128)(2,1)S(1)}, bf16[192,512]{1,0:T(8,128)(2,1)S(1)}, u32[]{:S(2)}, u32[]{:S(2)}) collective-permute-start(bf16[192,512]{1,0:T(8,128)(2,1)S(1)} %get-tuple-element.34.refs_1_.refs_5_), channel_id=1, source_target_pairs={{0,6},{2,0},{4,2},{6,4},{1,7},{3,1},{5,3},{7,5},{8,14},{10,8},{12,... | collective-permute-start | bytes 589832 | tf_op jit(solution)/shard_map/ppermute | solution.py:32
  253.1 8.5 %collective-permute-start.27 = (bf16[192,512]{1,0:T(8,128)(2,1)S(1)}, bf16[192,512]{1,0:T(8,128)(2,1)S(1)}, u32[]{:S(2)}, u32[]{:S(2)}) collective-permute-start(bf16[192,512]{1,0:T(8,128)(2,1)S(1)} %get-tuple-element.34.refs_1_.refs_5_), channel_id=1, source_target_pairs={{0,2},{2,4},{4,6},{6,0},{1,3},{3,5},{5,7},{7,1},{8,10},{10,12},{12... | collective-permute-start | bytes 589832 | tf_op jit(solution)/shard_map/ppermute | solution.py:32
  283.0 8.7 %collective-permute-start.34 = (bf16[208,512]{1,0:T(8,128)(2,1)S(1)}, bf16[208,512]{1,0:T(8,128)(2,1)S(1)}, u32[]{:S(2)}, u32[]{:S(2)}) collective-permute-start(bf16[208,512]{1,0:T(8,128)(2,1)S(1)} %conv.4.refs_0_), channel_id=1, source_target_pairs={{0,2},{2,4},{4,6},{6,0},{1,3},{3,5},{5,7},{7,1},{8,10},{10,12},{12... | collective-permute-start | bytes 638984 | tf_op jit(solution)/shard_map/ppermute | solution.py:32
  284.0 10.0 %collective-permute-start.35 = (bf16[208,512]{1,0:T(8,128)(2,1)S(1)}, bf16[208,512]{1,0:T(8,128)(2,1)S(1)}, u32[]{:S(2)}, u32[]{:S(2)}) collective-permute-start(bf16[208,512]{1,0:T(8,128)(2,1)S(1)} %conv.4.refs_0_), channel_id=1, source_target_pairs={{0,4},{2,6},{4,0},{6,2},{1,5},{3,7},{5,1},{7,3},{8,12},{10,14},{12... | collective-permute-start | bytes 638984 | tf_op jit(solution)/shard_map/ppermute | solution.py:32
  298.1 8.6 %collective-permute-start.37 = (bf16[192,512]{1,0:T(8,128)(2,1)S(1)}, bf16[192,512]{1,0:T(8,128)(2,1)S(1)}, u32[]{:S(2)}, u32[]{:S(2)}) collective-permute-start(bf16[192,512]{1,0:T(8,128)(2,1)S(1)} %get-tuple-element.38.refs_0_.refs_4_), channel_id=1, source_target_pairs={{0,2},{2,4},{4,6},{6,0},{1,3},{3,5},{5,7},{7,1},{8,10},{10,12},{12... | collective-permute-start | bytes 589832 | tf_op jit(solution)/shard_map/ppermute | solution.py:32
  298.6 8.1 %collective-permute-start.40 = (bf16[192,512]{1,0:T(8,128)(2,1)S(1)}, bf16[192,512]{1,0:T(8,128)(2,1)S(1)}, u32[]{:S(2)}, u32[]{:S(2)}) collective-permute-start(bf16[192,512]{1,0:T(8,128)(2,1)S(1)} %get-tuple-element.39.refs_1_.refs_5_), channel_id=1, source_target_pairs={{0,6},{2,0},{4,2},{6,4},{1,7},{3,1},{5,3},{7,5},{8,14},{10,8},{12,... | collective-permute-start | bytes 589832 | tf_op jit(solution)/shard_map/ppermute | solution.py:32
  301.4 8.8 %collective-permute-start.38 = (bf16[192,512]{1,0:T(8,128)(2,1)S(1)}, bf16[192,512]{1,0:T(8,128)(2,1)S(1)}, u32[]{:S(2)}, u32[]{:S(2)}) collective-permute-start(bf16[192,512]{1,0:T(8,128)(2,1)S(1)} %get-tuple-element.39.refs_1_.refs_5_), channel_id=1, source_target_pairs={{0,2},{2,4},{4,6},{6,0},{1,3},{3,5},{5,7},{7,1},{8,10},{10,12},{12... | collective-permute-start | bytes 589832 | tf_op jit(solution)/shard_map/ppermute | solution.py:32
  301.4 8.8 %collective-permute-start.42 = (bf16[192,512]{1,0:T(8,128)(2,1)S(1)}, bf16[192,512]{1,0:T(8,128)(2,1)S(1)}, u32[]{:S(2)}, u32[]{:S(2)}) collective-permute-start(bf16[192,512]{1,0:T(8,128)(2,1)S(1)} %get-tuple-element.38.refs_0_.refs_4_), channel_id=1, source_target_pairs={{0,6},{2,0},{4,2},{6,4},{1,7},{3,1},{5,3},{7,5},{8,14},{10,8},{12,... | collective-permute-start | bytes 589832 | tf_op jit(solution)/shard_map/ppermute | solution.py:32
  328.1 8.6 %collective-permute-start.45 = (bf16[208,512]{1,0:T(8,128)(2,1)S(1)}, bf16[208,512]{1,0:T(8,128)(2,1)S(1)}, u32[]{:S(2)}, u32[]{:S(2)}) collective-permute-start(bf16[208,512]{1,0:T(8,128)(2,1)S(1)} %conv.5.refs_0_), channel_id=1, source_target_pairs={{0,2},{2,4},{4,6},{6,0},{1,3},{3,5},{5,7},{7,1},{8,10},{10,12},{12... | collective-permute-start | bytes 638984 | tf_op jit(solution)/shard_map/ppermute | solution.py:32
  328.2 11.1 %collective-permute-start.46 = (bf16[208,512]{1,0:T(8,128)(2,1)S(1)}, bf16[208,512]{1,0:T(8,128)(2,1)S(1)}, u32[]{:S(2)}, u32[]{:S(2)}) collective-permute-start(bf16[208,512]{1,0:T(8,128)(2,1)S(1)} %conv.5.refs_0_), channel_id=1, source_target_pairs={{0,4},{2,6},{4,0},{6,2},{1,5},{3,7},{5,1},{7,3},{8,12},{10,14},{12... | collective-permute-start | bytes 638984 | tf_op jit(solution)/shard_map/ppermute | solution.py:32
  (49 other events, 676.5 us)
Sparse Core Ops, SparseCore 0:
  10.6 72.7 all-gather.4
  85.5 60.9 all-gather.6
